TPU v7x, 32 devices: a whole 2x2x4 slice. The times are simulated.
32 devices in a mesh: tp: 16 (over z, y, x), dp: 2 (over core).
Axes of the slice: x: 2, y: 2, z: 4, core: 2. Of those that a mesh axis runs over, the one named last changes fastest.
Arguments:
- tokens: bfloat16 [256, 4096], P(None, 'dp'), may hold values from -20 to 20
- norm_gain: float32 [2, 4096], P(None, 'dp'), may hold values from 0.1 to 1.9
- receptance: bfloat16 [2, 4096, 1024], P(None, 'dp', 'tp'), may hold values from -0.09375 to 0.09375
- key_proj: bfloat16 [2, 4096, 1024], P(None, 'dp', 'tp'), may hold values from -0.09375 to 0.09375
- value_proj: bfloat16 [2, 4096, 1024], P(None, 'dp', 'tp'), may hold values from -0.09375 to 0.09375
- decay_proj: bfloat16 [2, 4096, 1024], P(None, 'dp', 'tp'), may hold values from -0.09375 to 0.09375
- rate_proj: bfloat16 [2, 4096, 1024], P(None, 'dp', 'tp'), may hold values from -0.09375 to 0.09375
- gate_proj: bfloat16 [2, 4096, 1024], P(None, 'dp', 'tp'), may hold values from -0.09375 to 0.09375
- decay_base: float32 [2, 1024], P(None, 'tp'), may hold values from -6 to 1
- group_gain: float32 [2, 1024], P(None, 'tp'), may hold values from 0.1 to 1.9
- output_proj: bfloat16 [2, 1024, 4096], P(None, 'tp', 'dp'), may hold values from -0.1875 to 0.1875
- state: float32 [2, 256, 16, 4096], P(None, 'dp', 'tp'), may hold values from -3 to 3
Outputs:
- next_tokens: bfloat16 [256, 4096], P(None, 'dp')
- new_state: float32 [2, 256, 16, 4096], P(None, 'dp', 'tp')
All inputs are finite; a program needn't handle non-finite values.
Results may differ from a plain program's by a relative error of at most 0.0066.
Values may be sent and summed in bfloat16 or wider, within the bound.
No kernel may reach another device: no remote copies, remote signals or barrier semaphores. Data moves between devices by JAX's collectives and lax.ppermute only.
A program may use at most 64 MiB of HBM per device.

v0:
```python
import jax
import jax.numpy as jnp
from jax import lax
from jax.sharding import PartitionSpec as P

D = 4096
HEAD = 64
LAYERS = 2
norm_floor = 0.1
group_floor = 0.5


def recurrence(state_block, recept_heads, key_heads, value_heads, decay_heads, rate_heads):
    log_rate = -jax.nn.softplus(-decay_heads) - 0.5
    forget = jnp.exp(-jnp.exp(log_rate))
    learn_rate = jax.nn.sigmoid(rate_heads)
    unit_key = key_heads * lax.rsqrt(jnp.sum(key_heads * key_heads, axis=-1, keepdims=True) + 1.0)
    scaled = key_heads * learn_rate
    removed = jnp.einsum("bhvk,bhk->bhv", state_block, -unit_key, precision=lax.Precision.HIGHEST)
    updated = (
        state_block * forget[:, :, None, :]
        + removed[..., None] * (unit_key * learn_rate)[:, :, None, :]
        + value_heads[..., None] * scaled[:, :, None, :]
    )
    read_out = jnp.einsum("bhvk,bhk->bhv", updated, recept_heads, precision=lax.Precision.HIGHEST)
    centre = read_out - jnp.mean(read_out, axis=-1, keepdims=True)
    normal = centre * lax.rsqrt(jnp.mean(centre * centre, axis=-1, keepdims=True) + group_floor)
    return (updated, normal)


def shards(
    tokens,
    norm_gain,
    receptance,
    key_proj,
    value_proj,
    decay_proj,
    rate_proj,
    gate_proj,
    decay_base,
    group_gain,
    output_proj,
    state,
):
    local_rows = state.shape[1]
    first_row = lax.axis_index("dp") * local_rows
    local_heads = state.shape[2]
    current = tokens
    finals = []
    for section_index in range(LAYERS):
        floats = current.astype(jnp.float32)
        squares = jnp.sum(floats * floats, axis=1)
        normed = (floats * norm_gain[section_index]).astype(jnp.bfloat16)
        part_recept = jnp.dot(normed, receptance[section_index], preferred_element_type=jnp.float32)
        part_key = jnp.dot(normed, key_proj[section_index], preferred_element_type=jnp.float32)
        part_value = jnp.dot(normed, value_proj[section_index], preferred_element_type=jnp.float32)
        part_decay = jnp.dot(normed, decay_proj[section_index], preferred_element_type=jnp.float32)
        part_rate = jnp.dot(normed, rate_proj[section_index], preferred_element_type=jnp.float32)
        part_gate = jnp.dot(normed, gate_proj[section_index], preferred_element_type=jnp.float32)
        totals = lax.psum(squares, "dp")
        own_squares = lax.dynamic_slice_in_dim(totals, first_row, local_rows, 0)
        summed = (
            lax.psum_scatter(part_recept, "dp", scatter_dimension=0, tiled=True),
            lax.psum_scatter(part_key, "dp", scatter_dimension=0, tiled=True),
            lax.psum_scatter(part_value, "dp", scatter_dimension=0, tiled=True),
            lax.psum_scatter(part_decay, "dp", scatter_dimension=0, tiled=True),
            lax.psum_scatter(part_rate, "dp", scatter_dimension=0, tiled=True),
            lax.psum_scatter(part_gate, "dp", scatter_dimension=0, tiled=True),
        )
        inv_rms = lax.rsqrt(own_squares / D + norm_floor)

        def by_head(term):
            rounded = lax.optimization_barrier((inv_rms[:, None] * term).astype(jnp.bfloat16))
            return rounded.astype(jnp.float32).reshape(local_rows, local_heads, HEAD)

        decay_heads = by_head(summed[3]) + decay_base[section_index].reshape(1, local_heads, HEAD)
        updated, normal = recurrence(
            state[section_index].reshape(local_rows, local_heads, HEAD, HEAD),
            by_head(summed[0]),
            by_head(summed[1]),
            by_head(summed[2]),
            decay_heads,
            by_head(summed[4]),
        )
        finals.append(updated.reshape(local_rows, local_heads, HEAD * HEAD))
        gate_value = jax.nn.sigmoid(by_head(summed[5]).reshape(local_rows, local_heads * HEAD))
        mixed_heads = (
            normal.reshape(local_rows, local_heads * HEAD) * group_gain[section_index] * gate_value
        ).astype(jnp.bfloat16)
        weights_out = output_proj[section_index]

        def apply_out(piece, begin, weights_out=weights_out):
            return jnp.dot(piece, weights_out, preferred_element_type=jnp.float32)

        partial_out = apply_out(lax.all_gather(mixed_heads, "dp", axis=0, tiled=True), jnp.int32(0))
        total = lax.psum(partial_out, "tp")
        current = (floats + total).astype(jnp.bfloat16)
    return (current, jnp.stack(finals))


def solution(mesh):
    return jax.shard_map(
        shards,
        mesh=mesh,
        in_specs=(
            P(None, "dp"),
            P(None, "dp"),
            P(None, "dp", "tp"),
            P(None, "dp", "tp"),
            P(None, "dp", "tp"),
            P(None, "dp", "tp"),
            P(None, "dp", "tp"),
            P(None, "dp", "tp"),
            P(None, "tp"),
            P(None, "tp"),
            P(None, "tp", "dp"),
            P(None, "dp", "tp", None),
        ),
        out_specs=(P(None, "dp"), P(None, "dp", "tp", None)),
        check_vma=False,
    )
```

profile of v0, /device:TPU:0, one launch (start us, length us, event | category | flops | bytes accessed | tf_op | source)
XLA Modules:
  0.0 421.7 jit_solution(14630838087907600654)
XLA Ops:
  7.2 0.9 fusion.78
  8.1 2.3 fusion.22
  10.5 0.0 reduce-scatter.15.cloned.1.call-start
  10.5 2.4 fusion.26
  13.0 1.1 fusion.24
  14.1 1.1 fusion.20
  15.3 1.1 fusion.18
  16.4 0.0 reduce-scatter.13.cloned.1.call-start
  16.5 1.1 fusion.28
  17.6 8.1 %fusion.77 = (f32[1,128,1,4096]{3,2,1,0:T(1,128)}, f32[1,128,1,4096]{3,2,1,0:T(1,128)}) fusion(f32[2,128,1,4096]{3,2,1,0:T(1,128)} %param.23), kind=kLoop, calls=%fused_computation.119 | loop fusion | bytes 8388608 | tf_op jit(solution)/shard_map/slice | solution.py:78
  25.7 0.3 fusion
  26.0 5.0 %copy.45 = f32[1,128,1,4096]{1,3,2,0:T(8,128)S(1)} copy(f32[1,128,1,4096]{3,2,1,0:T(1,128)} %get-tuple-element.7) | data formatting | bytes 4194304
  31.1 2.6 psum.28
  33.7 0.1 add_rsqrt_fusion.5
  33.8 9.1 %reduce-scatter.17.cloned.1.call-done = f32[128,64]{0,1:T(8,128)} async-done(((f32[256,64]{0,1:T(8,128)}), f32[128,64]{0,1:T(8,128)}) %reduce-scatter.17.cloned.1.call-update) | async-done | bytes 32784 | tf_op jit(solution)/shard_map/reduce_scatter | solution.py:67
  42.8 10.7 %reduce-scatter.21.cloned.1.call-done = f32[128,64]{0,1:T(8,128)} async-done(((f32[256,64]{0,1:T(8,128)}), f32[128,64]{0,1:T(8,128)}) %reduce-scatter.21.cloned.1.call-update) | async-done | bytes 32784 | tf_op jit(solution)/shard_map/reduce_scatter | solution.py:63
  53.6 10.7 %reduce-scatter.23.cloned.1.call-done = f32[128,64]{0,1:T(8,128)} async-done(((f32[256,64]{0,1:T(8,128)}), f32[128,64]{0,1:T(8,128)}) %reduce-scatter.23.cloned.1.call-update) | async-done | bytes 32784 | tf_op jit(solution)/shard_map/reduce_scatter | solution.py:68
  64.3 10.7 %reduce-scatter.13.cloned.1.call-done = f32[128,64]{0,1:T(8,128)} async-done(((f32[256,64]{0,1:T(8,128)}), f32[128,64]{0,1:T(8,128)}) %reduce-scatter.13.cloned.1.call-update) | async-done | bytes 32784 | tf_op jit(solution)/shard_map/reduce_scatter | solution.py:66
  75.1 0.9 multiply_convert_fusion.10
  76.0 0.1 fusion.70
  76.1 0.3 multiply_reduce_fusion.3
  76.5 0.7 multiply_reduce_fusion.2
  77.3 0.1 multiply_convert_fusion.7
  77.4 1.9 all_gather.6
  79.2 2.7 fusion.38
  82.0 5.6 %copy.46 = f32[1,128,1,4096]{1,3,2,0:T(8,128)} copy(f32[1,128,1,4096]{3,2,1,0:T(1,128)} %get-tuple-element.6) | data formatting | bytes 4194304
  87.7 122.2 %all-reduce.3.cloned.1.call-done = f32[256,2048]{1,0:T(8,128)} async-done(((f32[256,2048]{1,0:T(8,128)}), f32[256,2048]{1,0:T(8,128)}) %all-reduce.3.cloned.1.call-update) | async-done | bytes 2097168 | tf_op jit(solution)/shard_map/psum | solution.py:96
  209.9 2.0 fusion.3
  211.9 1.0 copy-done.4
  212.9 1.1 fusion.10
  214.0 0.0 reduce-scatter.27.cloned.1.call-start
  214.0 2.4 fusion.14
  216.5 2.3 fusion.12
  218.9 0.0 reduce-scatter.33.cloned.1.call-start
  218.9 2.0 fusion.8
  221.0 0.0 reduce-scatter.35.cloned.1.call-start
  221.1 2.0 fusion.6
  223.1 2.0 fusion.16
  225.2 2.6 broadcast_multiply_fusion.2
  227.8 2.6 psum.30
  230.5 0.1 add_rsqrt_fusion.2
  230.5 1.3 reduce-scatter.27.cloned.1.call-done
  231.9 10.7 %reduce-scatter.29.cloned.1.call-done = f32[128,64]{0,1:T(8,128)} async-done(((f32[256,64]{0,1:T(8,128)}), f32[128,64]{0,1:T(8,128)}) %reduce-scatter.29.cloned.1.call-update) | async-done | bytes 32784 | tf_op jit(solution)/shard_map/reduce_scatter | solution.py:67
  242.6 11.5 %reduce-scatter.33.cloned.1.call-done = f32[128,64]{0,1:T(8,128)} async-done(((f32[256,64]{0,1:T(8,128)}), f32[128,64]{0,1:T(8,128)}) %reduce-scatter.33.cloned.1.call-update) | async-done | bytes 32784 | tf_op jit(solution)/shard_map/reduce_scatter | solution.py:63
  254.1 10.7 %reduce-scatter.35.cloned.1.call-done = f32[128,64]{0,1:T(8,128)} async-done(((f32[256,64]{0,1:T(8,128)}), f32[128,64]{0,1:T(8,128)}) %reduce-scatter.35.cloned.1.call-update) | async-done | bytes 32784 | tf_op jit(solution)/shard_map/reduce_scatter | solution.py:68
  264.8 10.9 %reduce-scatter.25.cloned.1.call-done = f32[128,64]{0,1:T(8,128)} async-done(((f32[256,64]{0,1:T(8,128)}), f32[128,64]{0,1:T(8,128)}) %reduce-scatter.25.cloned.1.call-update) | async-done | bytes 32784 | tf_op jit(solution)/shard_map/reduce_scatter | solution.py:66
  275.7 1.0 multiply_convert_fusion.3
  276.8 0.1 fusion.75
  276.9 1.9 multiply_reduce_fusion.1
  278.9 0.8 multiply_reduce_fusion
  279.7 0.1 multiply_convert_fusion
  279.8 1.9 all_gather.7
  281.7 2.7 fusion.30
  284.4 0.2 mul.342
  284.7 1.3 copy-done.2
  286.0 2.1 add_add_fusion.1
  288.2 0.4 broadcast_multiply_fusion
  288.5 0.2 mul.373
  288.8 1.3 copy-done.1
  290.1 0.6 add_add_fusion
  290.8 2.2 pad_maximum_fusion
  292.9 10.1 %copy.24 = f32[2,128,1,4096]{3,2,1,0:T(1,128)} copy(f32[2,128,1,4096]{1,3,2,0:T(8,128)} %pad_maximum_fusion) | data formatting | bytes 8388608
  303.1 109.3 %all-reduce.5.cloned.1.call-done = f32[256,2048]{1,0:T(8,128)} async-done(((f32[256,2048]{1,0:T(8,128)}), f32[256,2048]{1,0:T(8,128)}) %all-reduce.5.cloned.1.call-update) | async-done | bytes 2097168 | tf_op jit(solution)/shard_map/psum | solution.py:96
  412.4 2.8 fusion.5
  (69 shorter events, 0.9 us)
Async XLA Ops:
  7.2 5.8 %copy-start.3 = (bf16[256,2048]{1,0:T(8,128)(2,1)S(1)}, bf16[256,2048]{1,0:T(8,128)(2,1)}, u32[]{:S(2)}) copy-start(bf16[256,2048]{1,0:T(8,128)(2,1)} %param.12) | copy-start | bytes 3145732
  7.2 5.8 %copy-start.9 = (bf16[2,2048,64]{1,2,0:T(8,128)(2,1)S(1)}, bf16[2,2048,64]{1,2,0:T(8,128)(2,1)}, u32[]{:S(2)}) copy-start(bf16[2,2048,64]{1,2,0:T(8,128)(2,1)} %param.18) | copy-start | bytes 1572868
  7.2 26.6 %reduce-scatter.19.cloned.1.call-start = ((), (), s32[]{:S(2)}) async-start(), calls=%async_computation.15 | async-start | bytes 98304 | tf_op jit(solution)/shard_map/reduce_scatter | solution.py:65
  10.4 3.7 copy-start.10
  10.5 23.3 %reduce-scatter.15.cloned.1.call-start = ((), (), s32[]{:S(2)}) async-start(), calls=%async_computation.13 | async-start | bytes 98304 | tf_op jit(solution)/shard_map/reduce_scatter | solution.py:64
  12.9 2.4 copy-start.11
  12.9 29.9 %reduce-scatter.17.cloned.1.call-start = ((), (), s32[]{:S(2)}) async-start(), calls=%async_computation.14 | async-start | bytes 98304 | tf_op jit(solution)/shard_map/reduce_scatter | solution.py:67
  14.1 2.4 copy-start.12
  14.1 39.5 %reduce-scatter.21.cloned.1.call-start = ((), (), s32[]{:S(2)}) async-start(), calls=%async_computation.16 | async-start | bytes 98304 | tf_op jit(solution)/shard_map/reduce_scatter | solution.py:63
  15.2 49.1 %reduce-scatter.23.cloned.1.call-start = ((), (), s32[]{:S(2)}) async-start(), calls=%async_computation.17 | async-start | bytes 98304 | tf_op jit(solution)/shard_map/reduce_scatter | solution.py:68
  16.4 58.7 %reduce-scatter.13.cloned.1.call-start = ((), (), s32[]{:S(2)}) async-start(), calls=%async_computation.12 | async-start | bytes 98304 | tf_op jit(solution)/shard_map/reduce_scatter | solution.py:66
  17.5 8.2 %copy-start.6 = (f32[2,64]{1,0:T(2,128)S(1)}, f32[2,64]{1,0:T(2,128)}, u32[]{:S(2)}) copy-start(f32[2,64]{1,0:T(2,128)} %param.20) | copy-start | bytes 1540
  17.6 8.1 %copy-start.7 = (f32[2,64]{1,0:T(2,128)S(1)}, f32[2,64]{1,0:T(2,128)}, u32[]{:S(2)}) copy-start(f32[2,64]{1,0:T(2,128)} %param.21) | copy-start | bytes 1540
  17.6 192.3 %all-reduce.3.cloned.1.call-start = ((), (), s32[]{:S(2)}) async-start(), calls=%async_computation.18 | async-start | bytes 4194304 | tf_op jit(solution)/shard_map/psum | solution.py:96
  82.0 148.6 %reduce-scatter.31.cloned.1.call-start = ((), (), s32[]{:S(2)}) async-start(), calls=%async_computation.22 | async-start | bytes 98304 | tf_op jit(solution)/shard_map/reduce_scatter | solution.py:65
  209.9 3.0 copy-start.8
  211.9 1.0 copy-start.4
  214.0 5.0 %copy-start.5 = (bf16[256,2048]{1,0:T(8,128)(2,1)S(1)}, bf16[256,2048]{1,0:T(8,128)(2,1)}, u32[]{:S(2)}) copy-start(bf16[256,2048]{1,0:T(8,128)(2,1)} %copy-done.4) | copy-start | bytes 3145732
  214.0 17.9 %reduce-scatter.27.cloned.1.call-start = ((), (), s32[]{:S(2)}) async-start(), calls=%async_computation.20 | async-start | bytes 98304 | tf_op jit(solution)/shard_map/reduce_scatter | solution.py:64
  216.5 26.1 %reduce-scatter.29.cloned.1.call-start = ((), (), s32[]{:S(2)}) async-start(), calls=%async_computation.21 | async-start | bytes 98304 | tf_op jit(solution)/shard_map/reduce_scatter | solution.py:67
  218.9 35.2 %reduce-scatter.33.cloned.1.call-start = ((), (), s32[]{:S(2)}) async-start(), calls=%async_computation.23 | async-start | bytes 98304 | tf_op jit(solution)/shard_map/reduce_scatter | solution.py:63
  221.0 43.8 %reduce-scatter.35.cloned.1.call-start = ((), (), s32[]{:S(2)}) async-start(), calls=%async_computation.24 | async-start | bytes 98304 | tf_op jit(solution)/shard_map/reduce_scatter | solution.py:68
  223.1 52.6 %reduce-scatter.25.cloned.1.call-start = ((), (), s32[]{:S(2)}) async-start(), calls=%async_computation.19 | async-start | bytes 98304 | tf_op jit(solution)/shard_map/reduce_scatter | solution.py:66
  225.2 187.2 %all-reduce.5.cloned.1.call-start = ((), (), s32[]{:S(2)}) async-start(), calls=%async_computation.25 | async-start | bytes 4194304 | tf_op jit(solution)/shard_map/psum | solution.py:96
  275.7 3.2 copy-start
  284.4 1.6 copy-start.2
  288.5 1.6 copy-start.1
Sparse Core Ops, SparseCore 0:
  10.8 10.2 reduce-scatter.18
  23.2 8.6 reduce-scatter.14
  34.2 8.6 reduce-scatter.16
  44.9 8.6 reduce-scatter.20
  55.6 8.6 reduce-scatter.22
  66.4 8.6 reduce-scatter.12
  82.1 127.7 all-reduce.2
  214.1 6.7 reduce-scatter.30
  223.1 8.7 reduce-scatter.26
  233.9 8.6 reduce-scatter.28
  245.4 8.6 reduce-scatter.32
  256.1 8.6 reduce-scatter.34
  267.0 8.6 reduce-scatter.24
  284.6 127.7 all-reduce.4
where the time goes:
time: 423 us; the launch traced here: 422 us
  waiting for transfers between devices  318 us (75%)
  local copies, waits for them, and re-layouts  33.9 us (8%)
  matrix products  26.4 us (6%)
  other arithmetic  19.5 us (5%)
  between operations  14.2 us (3%)
  blocking collectives  8.96 us (2%)
    psum x2, waiting for transfers between devices, shards(): total = lax.psum(partial_out, 'tp')  231 us
    unnamed x29, local copies, waits for them, and re-layouts  24.5 us
    reduce_scatter x2, waiting for transfers between devices, shards(): lax.psum_scatter(part_recept, 'dp', scatter_dimension=0, tiled=True)  22.2 us
    reduce_scatter x2, waiting for transfers between devices, shards(): lax.psum_scatter(part_decay, 'dp', scatter_dimension=0, tiled=True)  21.6 us
    reduce_scatter x2, waiting for transfers between devices, shards(): lax.psum_scatter(part_gate, 'dp', scatter_dimension=0, tiled=True)  21.5 us
    reduce_scatter x2, waiting for transfers between devices, shards(): lax.psum_scatter(part_rate, 'dp', scatter_dimension=0, tiled=True)  19.8 us
  transfers between devices with their start and end apart: 14, of which 11 were waited for; matrix products, arithmetic and copies ran while one was open for 13% of the time, Pallas kernels for 0%

commit v1 on v0

--- a/solution.py
+++ b/solution.py
@@ -8,6 +8,14 @@
 LAYERS = 2
 norm_floor = 0.1
 group_floor = 0.5
+
+
+def sum_by_hops(x, axis):
+    size, result = (lax.axis_size(axis), x)
+    for stride in [1 << k for k in range(size.bit_length() - 1)]:
+        route = [(i, i ^ stride) for i in range(size)]
+        result = result + lax.ppermute(result, axis, route)
+    return result
 
 
 def recurrence(state_block, recept_heads, key_heads, value_heads, decay_heads, rate_heads):
@@ -93,7 +101,7 @@
             return jnp.dot(piece, weights_out, preferred_element_type=jnp.float32)
 
         partial_out = apply_out(lax.all_gather(mixed_heads, "dp", axis=0, tiled=True), jnp.int32(0))
-        total = lax.psum(partial_out, "tp")
+        total = sum_by_hops(partial_out, "tp")
         current = (floats + total).astype(jnp.bfloat16)
     return (current, jnp.stack(finals))
 

time: 423 us -> 634 us (1.50)
  waiting for transfers between devices: 318 us -> 519 us
  starting transfers between devices: 0.58 us -> 16.7 us
    ppermute x0 -> x8, waiting for transfers between devices: none -> 433 us  [sum_by_hops(): result = result + lax.ppermute(result, axis, route)]
    psum x2 -> x0, waiting for transfers between devices: 231 us -> none  [shards(): total = lax.psum(partial_out, 'tp')]
    ppermute x0 -> x8, starting transfers between devices: none -> 16.1 us  [sum_by_hops(): result = result + lax.ppermute(result, axis, route)]
    unnamed x29 -> x27, local copies, waits for them, and re-layouts: 24.5 us -> 23.2 us
  transfers between devices with their start and end apart: 14 -> 20, of which waited for: 11 -> 17; matrix products, arithmetic and copies ran while one was open for 13% -> 8% of each run, Pallas kernels for 0% -> 0%
where the time goes in v1:
time: 634 us; the launch traced here: 633 us
  waiting for transfers between devices  519 us (82%)
  local copies, waits for them, and re-layouts  32.6 us (5%)
  matrix products  23.7 us (4%)
  other arithmetic  18.4 us (3%)
  starting transfers between devices  16.7 us (3%)
  between operations  14.5 us (2%)
  blocking collectives  8.78 us (1%)
    ppermute x8, waiting for transfers between devices, sum_by_hops(): result = result + lax.ppermute(result, axis, route)  433 us
    unnamed x27, local copies, waits for them, and re-layouts  23.2 us
    reduce_scatter x2, waiting for transfers between devices, shards(): lax.psum_scatter(part_recept, 'dp', scatter_dimension=0, tiled=True)  22 us
    reduce_scatter x2, waiting for transfers between devices, shards(): lax.psum_scatter(part_gate, 'dp', scatter_dimension=0, tiled=True)  21.6 us
    reduce_scatter x2, waiting for transfers between devices, shards(): lax.psum_scatter(part_decay, 'dp', scatter_dimension=0, tiled=True)  21.5 us
    reduce_scatter x2, waiting for transfers between devices, shards(): lax.psum_scatter(part_rate, 'dp', scatter_dimension=0, tiled=True)  20 us
    ppermute x8, starting transfers between devices, sum_by_hops(): result = result + lax.ppermute(result, axis, route)  16.1 us
  transfers between devices with their start and end apart: 20, of which 17 were waited for; matrix products, arithmetic and copies ran while one was open for 8% of the time, Pallas kernels for 0%

profile of v1, /device:TPU:0, one launch (start us, length us, event | category | flops | bytes accessed | tf_op | source)
XLA Modules:
  0.0 633.3 jit_solution(6865565624077744271)
XLA Ops:
  7.2 0.9 fusion.78
  8.1 2.3 fusion.22
  10.5 2.4 fusion.26
  13.0 1.1 fusion.24
  14.1 1.1 fusion.20
  15.3 1.1 fusion.18
  16.5 1.1 fusion.28
  17.6 8.1 %fusion.77 = (f32[1,128,1,4096]{3,2,1,0:T(1,128)}, f32[1,128,1,4096]{3,2,1,0:T(1,128)}) fusion(f32[2,128,1,4096]{3,2,1,0:T(1,128)} %param.23), kind=kLoop, calls=%fused_computation.119 | loop fusion | bytes 8388608 | tf_op jit(solution)/shard_map/slice | solution.py:86
  26.0 5.0 copy.45
  31.1 2.6 psum.14
  33.8 9.1 %reduce-scatter.17.cloned.1.call-done = f32[128,64]{0,1:T(8,128)} async-done(((f32[256,64]{0,1:T(8,128)}), f32[128,64]{0,1:T(8,128)}) %reduce-scatter.17.cloned.1.call-update) | async-done | bytes 32784 | tf_op jit(solution)/shard_map/reduce_scatter | solution.py:75
  42.8 10.7 %reduce-scatter.21.cloned.1.call-done = f32[128,64]{0,1:T(8,128)} async-done(((f32[256,64]{0,1:T(8,128)}), f32[128,64]{0,1:T(8,128)}) %reduce-scatter.21.cloned.1.call-update) | async-done | bytes 32784 | tf_op jit(solution)/shard_map/reduce_scatter | solution.py:71
  53.6 10.7 %reduce-scatter.23.cloned.1.call-done = f32[128,64]{0,1:T(8,128)} async-done(((f32[256,64]{0,1:T(8,128)}), f32[128,64]{0,1:T(8,128)}) %reduce-scatter.23.cloned.1.call-update) | async-done | bytes 32784 | tf_op jit(solution)/shard_map/reduce_scatter | solution.py:76
  64.3 10.7 %reduce-scatter.13.cloned.1.call-done = f32[128,64]{0,1:T(8,128)} async-done(((f32[256,64]{0,1:T(8,128)}), f32[128,64]{0,1:T(8,128)}) %reduce-scatter.13.cloned.1.call-update) | async-done | bytes 32784 | tf_op jit(solution)/shard_map/reduce_scatter | solution.py:74
  75.1 0.9 multiply_convert_fusion.10
  76.1 0.3 multiply_reduce_fusion.3
  76.5 0.7 multiply_reduce_fusion.2
  77.4 1.9 all_gather.6
  79.2 1.4 fusion.38
  80.6 1.7 collective-permute-start
  82.3 46.1 %collective-permute-done = f32[256,2048]{1,0:T(8,128)S(1)} collective-permute-done((f32[256,2048]{1,0:T(8,128)S(1)}, f32[256,2048]{1,0:T(8,128)S(1)}, u32[]{:S(2)}, u32[]{:S(2)}) %collective-permute-start) | collective-permute-done | bytes 2097184 | tf_op jit(solution)/shard_map/ppermute | solution.py:17
  128.5 0.3 add.197
  128.8 1.8 collective-permute-start.1
  130.6 45.3 %collective-permute-done.1 = f32[256,2048]{1,0:T(8,128)S(1)} collective-permute-done((f32[256,2048]{1,0:T(8,128)S(1)}, f32[256,2048]{1,0:T(8,128)S(1)}, u32[]{:S(2)}, u32[]{:S(2)}) %collective-permute-start.1) | collective-permute-done | bytes 2097184 | tf_op jit(solution)/shard_map/ppermute | solution.py:17
  176.2 1.8 collective-permute-start.2
  178.1 44.4 %collective-permute-done.2 = f32[256,2048]{1,0:T(8,128)S(1)} collective-permute-done((f32[256,2048]{1,0:T(8,128)S(1)}, f32[256,2048]{1,0:T(8,128)S(1)}, u32[]{:S(2)}, u32[]{:S(2)}) %collective-permute-start.2) | collective-permute-done | bytes 2097184 | tf_op jit(solution)/shard_map/ppermute | solution.py:17
  222.9 2.7 collective-permute-start.3
  225.6 88.5 %collective-permute-done.3 = f32[256,2048]{1,0:T(8,128)S(1)} collective-permute-done((f32[256,2048]{1,0:T(8,128)S(1)}, f32[256,2048]{1,0:T(8,128)S(1)}, u32[]{:S(2)}, u32[]{:S(2)}) %collective-permute-start.3) | collective-permute-done | bytes 2097184 | tf_op jit(solution)/shard_map/ppermute | solution.py:17
  314.1 0.6 fusion.3
  314.7 1.0 copy-done.3
  315.7 1.1 fusion.10
  316.8 2.4 fusion.14
  319.3 2.3 fusion.12
  321.7 2.0 fusion.8
  324.0 2.0 fusion.6
  326.1 2.0 fusion.16
  328.2 5.6 copy.46
  333.8 2.4 psum.15
  336.5 10.9 %reduce-scatter.29.cloned.1.call-done = f32[128,64]{0,1:T(8,128)} async-done(((f32[256,64]{0,1:T(8,128)}), f32[128,64]{0,1:T(8,128)}) %reduce-scatter.29.cloned.1.call-update) | async-done | bytes 32784 | tf_op jit(solution)/shard_map/reduce_scatter | solution.py:75
  347.4 11.3 %reduce-scatter.33.cloned.1.call-done = f32[128,64]{0,1:T(8,128)} async-done(((f32[256,64]{0,1:T(8,128)}), f32[128,64]{0,1:T(8,128)}) %reduce-scatter.33.cloned.1.call-update) | async-done | bytes 32784 | tf_op jit(solution)/shard_map/reduce_scatter | solution.py:71
  358.7 10.9 %reduce-scatter.35.cloned.1.call-done = f32[128,64]{0,1:T(8,128)} async-done(((f32[256,64]{0,1:T(8,128)}), f32[128,64]{0,1:T(8,128)}) %reduce-scatter.35.cloned.1.call-update) | async-done | bytes 32784 | tf_op jit(solution)/shard_map/reduce_scatter | solution.py:76
  369.6 10.7 %reduce-scatter.25.cloned.1.call-done = f32[128,64]{0,1:T(8,128)} async-done(((f32[256,64]{0,1:T(8,128)}), f32[128,64]{0,1:T(8,128)}) %reduce-scatter.25.cloned.1.call-update) | async-done | bytes 32784 | tf_op jit(solution)/shard_map/reduce_scatter | solution.py:74
  380.3 1.0 multiply_convert_fusion.3
  381.6 1.9 multiply_reduce_fusion.1
  383.5 0.8 multiply_reduce_fusion
  384.4 1.9 all_gather.7
  386.3 1.4 fusion.30
  387.7 1.8 collective-permute-start.4
  389.5 46.1 %collective-permute-done.4 = f32[256,2048]{1,0:T(8,128)S(1)} collective-permute-done((f32[256,2048]{1,0:T(8,128)S(1)}, f32[256,2048]{1,0:T(8,128)S(1)}, u32[]{:S(2)}, u32[]{:S(2)}) %collective-permute-start.4) | collective-permute-done | bytes 2097184 | tf_op jit(solution)/shard_map/ppermute | solution.py:17
  435.9 1.8 collective-permute-start.5
  437.8 45.3 %collective-permute-done.5 = f32[256,2048]{1,0:T(8,128)S(1)} collective-permute-done((f32[256,2048]{1,0:T(8,128)S(1)}, f32[256,2048]{1,0:T(8,128)S(1)}, u32[]{:S(2)}, u32[]{:S(2)}) %collective-permute-start.5) | collective-permute-done | bytes 2097184 | tf_op jit(solution)/shard_map/ppermute | solution.py:17
  483.4 1.8 collective-permute-start.6
  485.2 0.6 broadcast_multiply_fusion.2
  485.8 43.9 %collective-permute-done.6 = f32[256,2048]{1,0:T(8,128)S(1)} collective-permute-done((f32[256,2048]{1,0:T(8,128)S(1)}, f32[256,2048]{1,0:T(8,128)S(1)}, u32[]{:S(2)}, u32[]{:S(2)}) %collective-permute-start.6) | collective-permute-done | bytes 2097184 | tf_op jit(solution)/shard_map/ppermute | solution.py:17
  529.7 1.6 add.215
  531.2 2.6 collective-permute-start.7
  534.1 0.4 add_add_fusion.1
  534.5 0.4 broadcast_multiply_fusion
  535.1 1.3 copy-done.1
  536.4 0.6 add_add_fusion
  537.1 2.2 pad_maximum_fusion
  539.3 10.1 %copy.24 = f32[2,128,1,4096]{3,2,1,0:T(1,128)} copy(f32[2,128,1,4096]{1,3,2,0:T(8,128)} %pad_maximum_fusion) | data formatting | bytes 8388608
  549.4 73.3 %collective-permute-done.7 = f32[256,2048]{1,0:T(8,128)} collective-permute-done((f32[256,2048]{1,0:T(8,128)}, f32[256,2048]{1,0:T(8,128)}, u32[]{:S(2)}, u32[]{:S(2)}) %collective-permute-start.7) | collective-permute-done | bytes 2097184 | tf_op jit(solution)/shard_map/ppermute | solution.py:17
  622.7 3.7 fusion.5
  (83 shorter events, 4.0 us)
Async XLA Ops:
  7.2 5.8 copy-start.2
  7.2 5.8 copy-start.8
  7.2 26.6 %reduce-scatter.19.cloned.1.call-start = ((), (), s32[]{:S(2)}) async-start(), calls=%async_computation.15 | async-start | bytes 98304 | tf_op jit(solution)/shard_map/reduce_scatter | solution.py:73
  10.4 3.7 copy-start.9
  10.5 23.3 %reduce-scatter.15.cloned.1.call-start = ((), (), s32[]{:S(2)}) async-start(), calls=%async_computation.13 | async-start | bytes 98304 | tf_op jit(solution)/shard_map/reduce_scatter | solution.py:72
  12.9 2.4 copy-start.10
  12.9 29.9 %reduce-scatter.17.cloned.1.call-start = ((), (), s32[]{:S(2)}) async-start(), calls=%async_computation.14 | async-start | bytes 98304 | tf_op jit(solution)/shard_map/reduce_scatter | solution.py:75
  14.1 2.4 copy-start.11
  14.1 39.5 %reduce-scatter.21.cloned.1.call-start = ((), (), s32[]{:S(2)}) async-start(), calls=%async_computation.16 | async-start | bytes 98304 | tf_op jit(solution)/shard_map/reduce_scatter | solution.py:71
  15.2 49.1 %reduce-scatter.23.cloned.1.call-start = ((), (), s32[]{:S(2)}) async-start(), calls=%async_computation.17 | async-start | bytes 98304 | tf_op jit(solution)/shard_map/reduce_scatter | solution.py:76
  16.4 58.7 %reduce-scatter.13.cloned.1.call-start = ((), (), s32[]{:S(2)}) async-start(), calls=%async_computation.12 | async-start | bytes 98304 | tf_op jit(solution)/shard_map/reduce_scatter | solution.py:74
  17.5 8.2 %copy-start.5 = (f32[2,64]{1,0:T(2,128)S(1)}, f32[2,64]{1,0:T(2,128)}, u32[]{:S(2)}) copy-start(f32[2,64]{1,0:T(2,128)} %param.20) | copy-start | bytes 1540
  17.6 8.1 %copy-start.6 = (f32[2,64]{1,0:T(2,128)S(1)}, f32[2,64]{1,0:T(2,128)}, u32[]{:S(2)}) copy-start(f32[2,64]{1,0:T(2,128)} %param.21) | copy-start | bytes 1540
  17.6 318.8 %reduce-scatter.31.cloned.1.call-start = ((), (), s32[]{:S(2)}) async-start(), calls=%async_computation.21 | async-start | bytes 98304 | tf_op jit(solution)/shard_map/reduce_scatter | solution.py:73
  80.6 47.9 %collective-permute-start = (f32[256,2048]{1,0:T(8,128)S(1)}, f32[256,2048]{1,0:T(8,128)S(1)}, u32[]{:S(2)}, u32[]{:S(2)}) collective-permute-start(f32[256,2048]{1,0:T(8,128)S(1)} %fusion.38), channel_id=1, source_target_pairs={{0,2},{2,0},{4,6},{6,4},{8,10},{10,8},{12,14},{14,12},{16,18},{18,... | collective-permute-start | bytes 6291464 | tf_op jit(solution)/shard_map/ppermute | solution.py:17
  128.8 47.1 %collective-permute-start.1 = (f32[256,2048]{1,0:T(8,128)S(1)}, f32[256,2048]{1,0:T(8,128)S(1)}, u32[]{:S(2)}, u32[]{:S(2)}) collective-permute-start(f32[256,2048]{1,0:T(8,128)S(1)} %add.197), channel_id=1, source_target_pairs={{0,4},{2,6},{4,0},{6,2},{8,12},{10,14},{12,8},{14,10},{16,20},{18,... | collective-permute-start | bytes 6291464 | tf_op jit(solution)/shard_map/ppermute | solution.py:17
  176.2 46.3 %collective-permute-start.2 = (f32[256,2048]{1,0:T(8,128)S(1)}, f32[256,2048]{1,0:T(8,128)S(1)}, u32[]{:S(2)}, u32[]{:S(2)}) collective-permute-start(f32[256,2048]{1,0:T(8,128)S(1)} %add.198), channel_id=1, source_target_pairs={{0,8},{2,10},{4,12},{6,14},{8,0},{10,2},{12,4},{14,6},{16,24},{18,... | collective-permute-start | bytes 6291464 | tf_op jit(solution)/shard_map/ppermute | solution.py:17
  222.9 92.8 %copy-start.7 = (bf16[2,2048,64]{1,2,0:T(8,128)(2,1)S(1)}, bf16[2,2048,64]{1,2,0:T(8,128)(2,1)}, u32[]{:S(2)}) copy-start(bf16[2,2048,64]{1,2,0:T(8,128)(2,1)} %param.16) | copy-start | bytes 1572868
  222.9 91.2 %collective-permute-start.3 = (f32[256,2048]{1,0:T(8,128)S(1)}, f32[256,2048]{1,0:T(8,128)S(1)}, u32[]{:S(2)}, u32[]{:S(2)}) collective-permute-start(f32[256,2048]{1,0:T(8,128)S(1)} %add.199), channel_id=1, source_target_pairs={{0,16},{2,18},{4,20},{6,22},{8,24},{10,26},{12,28},{14,30},{16,0},... | collective-permute-start | bytes 6291464 | tf_op jit(solution)/shard_map/ppermute | solution.py:17
  314.7 1.0 copy-start.3
  316.8 5.0 copy-start.4
  316.8 19.7 %reduce-scatter.27.cloned.1.call-start = ((), (), s32[]{:S(2)}) async-start(), calls=%async_computation.19 | async-start | bytes 98304 | tf_op jit(solution)/shard_map/reduce_scatter | solution.py:72
  319.3 28.1 %reduce-scatter.29.cloned.1.call-start = ((), (), s32[]{:S(2)}) async-start(), calls=%async_computation.20 | async-start | bytes 98304 | tf_op jit(solution)/shard_map/reduce_scatter | solution.py:75
  321.7 37.0 %reduce-scatter.33.cloned.1.call-start = ((), (), s32[]{:S(2)}) async-start(), calls=%async_computation.22 | async-start | bytes 98304 | tf_op jit(solution)/shard_map/reduce_scatter | solution.py:71
  323.8 45.8 %reduce-scatter.35.cloned.1.call-start = ((), (), s32[]{:S(2)}) async-start(), calls=%async_computation.23 | async-start | bytes 98304 | tf_op jit(solution)/shard_map/reduce_scatter | solution.py:76
  326.1 54.3 %reduce-scatter.25.cloned.1.call-start = ((), (), s32[]{:S(2)}) async-start(), calls=%async_computation.18 | async-start | bytes 98304 | tf_op jit(solution)/shard_map/reduce_scatter | solution.py:74
  380.3 3.2 copy-start
  387.7 47.9 %collective-permute-start.4 = (f32[256,2048]{1,0:T(8,128)S(1)}, f32[256,2048]{1,0:T(8,128)S(1)}, u32[]{:S(2)}, u32[]{:S(2)}) collective-permute-start(f32[256,2048]{1,0:T(8,128)S(1)} %fusion.30), channel_id=1, source_target_pairs={{0,2},{2,0},{4,6},{6,4},{8,10},{10,8},{12,14},{14,12},{16,18},{18,... | collective-permute-start | bytes 6291464 | tf_op jit(solution)/shard_map/ppermute | solution.py:17
  435.9 47.1 %collective-permute-start.5 = (f32[256,2048]{1,0:T(8,128)S(1)}, f32[256,2048]{1,0:T(8,128)S(1)}, u32[]{:S(2)}, u32[]{:S(2)}) collective-permute-start(f32[256,2048]{1,0:T(8,128)S(1)} %add.213), channel_id=1, source_target_pairs={{0,4},{2,6},{4,0},{6,2},{8,12},{10,14},{12,8},{14,10},{16,20},{18,... | collective-permute-start | bytes 6291464 | tf_op jit(solution)/shard_map/ppermute | solution.py:17
  483.4 46.3 %collective-permute-start.6 = (f32[256,2048]{1,0:T(8,128)S(1)}, f32[256,2048]{1,0:T(8,128)S(1)}, u32[]{:S(2)}, u32[]{:S(2)}) collective-permute-start(f32[256,2048]{1,0:T(8,128)S(1)} %add.214), channel_id=1, source_target_pairs={{0,8},{2,10},{4,12},{6,14},{8,0},{10,2},{12,4},{14,6},{16,24},{18,... | collective-permute-start | bytes 6291464 | tf_op jit(solution)/shard_map/ppermute | solution.py:17
  531.2 91.5 %collective-permute-start.7 = (f32[256,2048]{1,0:T(8,128)}, f32[256,2048]{1,0:T(8,128)}, u32[]{:S(2)}, u32[]{:S(2)}) collective-permute-start(f32[256,2048]{1,0:T(8,128)} %add.215), channel_id=1, source_target_pairs={{0,16},{2,18},{4,20},{6,22},{8,24},{10,26},{12,28},{14,30},{16,0},... | collective-permute-start | bytes 6291464 | tf_op jit(solution)/shard_map/ppermute | solution.py:17
  534.8 1.6 copy-start.1
Sparse Core Ops, SparseCore 0:
  10.8 10.2 reduce-scatter.18
  23.2 8.6 reduce-scatter.14
  34.2 8.6 reduce-scatter.16
  44.9 8.6 reduce-scatter.20
  55.6 8.6 reduce-scatter.22
  66.4 8.6 reduce-scatter.12
  316.9 8.6 reduce-scatter.30
  327.8 8.7 reduce-scatter.26
  338.7 8.6 reduce-scatter.28
  350.0 8.6 reduce-scatter.32
  360.9 8.6 reduce-scatter.34
  371.6 8.6 reduce-scatter.24
